TPU v7x, 256 devices: a whole 4x4x8 slice. The times are simulated.
256 devices in a mesh: rep: 2 (over z_hi), fs: 16 (over z_lo, y), tp: 8 (over x, core).
Axes of the slice: x: 4, y: 4, z: 8 (z_hi: 2, z_lo: 4; z = z_hi * 4 + z_lo), core: 2. Of those that a mesh axis runs over, the one named last changes fastest.
Arguments:
- stream: bfloat16 [16384, 2048], P(('rep', 'fs'), 'tp'), may hold values from -6 to 6
- recurrent_norm_gain: float32 [2048], replicated, may hold values from 0.1 to 1.9
- feedforward_norm_gain: float32 [2048], replicated, may hold values from 0.1 to 1.9
- recurrent_input_weight: bfloat16 [2048, 2048], P('fs', 'tp'), may hold values from -0.125 to 0.125
- output_gate_weight: bfloat16 [2048, 2048], P('fs', 'tp'), may hold values from -0.125 to 0.125
- causal_filter_weight: bfloat16 [4, 2048], P(None, 'tp'), may hold values from -3 to 3
- decay_gate_matrix: bfloat16 [32, 64, 64], P('tp'), may hold values from -0.75 to 0.75
- input_gate_matrix: bfloat16 [32, 64, 64], P('tp'), may hold values from -0.75 to 0.75
- channel_decay_param: float32 [2048], P('tp'), may hold values from 3 to 10
- token_decay_offset: float32 [16384, 2048], P(('rep', 'fs'), 'tp'), may hold values from -0.7 to 0, as said below
- recurrent_output_weight: bfloat16 [2048, 2048], P('tp', 'fs'), may hold values from -0.125 to 0.125
- up_projection_weight: bfloat16 [2048, 6144], P('fs', 'tp'), may hold values from -0.125 to 0.125
- down_projection_weight: bfloat16 [6144, 2048], P('tp', 'fs'), may hold values from -0.078125 to 0.078125
Outputs:
- updated: bfloat16 [16384, 2048], P(('rep', 'fs'), 'tp')
Inputs may be any that keep to these rules, and one draw needn't show every extreme that they name: `token_decay_offset`: zero except at a few positions, where a whole row is negative.
All inputs are finite; a program needn't handle non-finite values.
Results may differ from a plain program's by a relative error of at most 0.015.
Values may be sent and summed in bfloat16 or wider, within the bound.
A program may use at most 64 MiB of HBM per device.

v0:
```python
import jax
import jax.numpy as jnp
from jax import lax
from jax.sharding import Mesh
from jax.sharding import PartitionSpec as P

SEQ_LEN = 128
FS = ("fs_0", "fs_1")
REP_FS = ("rep", "fs_0", "fs_1")
EPSILON = 1e-06
DECAY_MULTIPLIER = 8.0


def in_order(pieces, dim):
    shape = list(pieces.shape[1:])
    shape[dim] *= pieces.shape[0]
    return jnp.moveaxis(pieces, 0, dim).reshape(shape)


def from_everyone(value, axis):
    copies = jnp.broadcast_to(value, (lax.axis_size(axis), *value.shape))
    return lax.all_to_all(copies, axis, split_axis=0, concat_axis=0, tiled=True)


def gather_directly(value, axis, dim):
    return in_order(from_everyone(value, axis), dim)


def in_one_piece(arrays, axis, dim, along):
    ends, at = ([], 0)
    for a in arrays[:-1]:
        at += a.shape[along]
        ends.append(at)
    both = jnp.concatenate(arrays, axis=along)
    return tuple(jnp.split(lax.all_gather(both, axis, axis=dim, tiled=True), ends, axis=along))


def split_up(value, dim, devices):
    before, after = (value.shape[:dim], value.shape[dim + 1 :])
    return jnp.moveaxis(value.reshape(*before, devices, -1, *after), dim, 0)


def sent_and_summed(value, axis, dim):
    pieces = split_up(value, dim, lax.axis_size(axis))
    arrived = lax.all_to_all(pieces, axis, split_axis=0, concat_axis=0, tiled=True)
    return arrived.astype(jnp.float32).sum(axis=0)


def gather_in_order(value, axes, order):
    pieces = value[None]
    for k in order:
        pieces = lax.all_gather(pieces, axes[k], axis=0, tiled=True)
    held = [lax.axis_size(axes[k]) for k in reversed(order)]
    pieces = pieces.reshape(*held, *value.shape)
    turned = sorted(range(len(order)), key=lambda place: order[len(order) - 1 - place])
    return pieces.transpose(*turned, *range(len(order), pieces.ndim)).reshape(-1, *value.shape)


def gather_axes(value, axes, order, dim):
    return in_order(gather_in_order(value, axes, order), dim)


def norm_rows(values, gain):
    widened = values.astype(jnp.float32)
    inverse = lax.rsqrt(jnp.mean(widened * widened, axis=-1, keepdims=True) + EPSILON)
    return (widened * inverse * gain).astype(jnp.bfloat16)


def short_filter(values, causal_filter_weight, sequence_length):
    positions, channels = values.shape
    sequences = positions // sequence_length
    reach = causal_filter_weight.shape[0]
    widened = (
        lax.optimization_barrier(values)
        .astype(jnp.float32)
        .reshape(sequences, sequence_length, channels)
    )
    padded = jnp.pad(widened, ((0, 0), (reach - 1, 0), (0, 0)))
    taps = causal_filter_weight.astype(jnp.float32)
    total = taps[0] * padded[:, 0:sequence_length]
    for offset in range(1, reach):
        total = total + taps[offset] * padded[:, offset : offset + sequence_length]
    return total.reshape(positions, channels).astype(jnp.bfloat16)


def combine(earlier, later):
    return (earlier[0] * later[0], later[0] * earlier[1] + later[1])


def recurrent_states(
    filtered_input,
    output_gate_rows,
    decay_gate_matrix,
    input_gate_matrix,
    channel_decay_param,
    token_decay_offset,
    sequence_length,
):
    positions, channels = filtered_input.shape
    blocks, block_size, _ = decay_gate_matrix.shape
    grouped = filtered_input.reshape(positions, blocks, block_size)
    recurrent_step = jax.nn.sigmoid(
        jnp.einsum(
            "tnc,ncd->tnd", grouped, decay_gate_matrix, preferred_element_type=jnp.float32
        ).reshape(positions, channels)
    )
    inputs = jax.nn.sigmoid(
        jnp.einsum(
            "tnc,ncd->tnd", grouped, input_gate_matrix, preferred_element_type=jnp.float32
        ).reshape(positions, channels)
    )
    decay_logarithm = (
        -DECAY_MULTIPLIER * recurrent_step * jax.nn.softplus(-channel_decay_param)
        + token_decay_offset
    )
    widened = lax.optimization_barrier(filtered_input).astype(jnp.float32)
    drive = jnp.sqrt(-jnp.expm1(2.0 * decay_logarithm)) * inputs * widened
    shaped = (positions // sequence_length, sequence_length, channels)
    _, states = lax.associative_scan(
        combine, (jnp.exp(decay_logarithm).reshape(shaped), drive.reshape(shaped)), axis=1
    )
    gate_wide = lax.optimization_barrier(output_gate_rows).astype(jnp.float32)
    return (states.reshape(positions, channels) * jax.nn.gelu(gate_wide, approximate=False)).astype(
        jnp.bfloat16
    )


def shards(
    stream,
    recurrent_norm_gain,
    feedforward_norm_gain,
    recurrent_input_weight,
    output_gate_weight,
    causal_filter_weight,
    decay_gate_matrix,
    input_gate_matrix,
    channel_decay_param,
    token_decay_offset,
    recurrent_output_weight,
    up_projection_weight,
    down_projection_weight,
):
    whole = gather_directly(stream, "tp", 1)
    normed = norm_rows(whole, recurrent_norm_gain)
    pieces = in_one_piece((recurrent_input_weight, output_gate_weight), FS, 0, 1)
    columns = normed
    value_total = jnp.dot(columns, pieces[0], preferred_element_type=jnp.float32)
    gate_total = jnp.dot(columns, pieces[1], preferred_element_type=jnp.float32)
    filtered_input = short_filter(value_total.astype(jnp.bfloat16), causal_filter_weight, SEQ_LEN)
    mixed_rows = recurrent_states(
        filtered_input,
        gate_total.astype(jnp.bfloat16),
        decay_gate_matrix,
        input_gate_matrix,
        channel_decay_param,
        token_decay_offset,
        SEQ_LEN,
    )
    mixer_terms = jnp.dot(
        mixed_rows,
        gather_directly(recurrent_output_weight, FS, 1),
        preferred_element_type=jnp.float32,
    )
    summed = sent_and_summed(mixer_terms.astype(jnp.bfloat16), "tp", 1)
    middle = (stream.astype(jnp.float32) + summed).astype(jnp.bfloat16)
    whole_mid = gather_directly(middle, "tp", 1)
    normed_mid = norm_rows(whole_mid, feedforward_norm_gain)
    columns = normed_mid
    raised = jnp.dot(
        columns,
        gather_axes(up_projection_weight, FS, (0, 1), 0),
        preferred_element_type=jnp.float32,
    )
    activity = jnp.square(jax.nn.relu(raised)).astype(jnp.bfloat16)
    channel_terms = jnp.dot(
        activity,
        gather_axes(down_projection_weight, FS, (0, 1), 1),
        preferred_element_type=jnp.float32,
    )
    channel_sum = sent_and_summed(channel_terms.astype(jnp.bfloat16), "tp", 1)
    return (middle.astype(jnp.float32) + channel_sum).astype(jnp.bfloat16)


def solution(mesh):
    split = Mesh(
        mesh.devices.reshape(mesh.shape["rep"], 4, 4, mesh.shape["tp"]),
        ("rep", "fs_0", "fs_1", "tp"),
    )
    placed = (
        P(REP_FS, "tp"),
        P(),
        P(),
        P(FS, "tp"),
        P(FS, "tp"),
        P(None, "tp"),
        P("tp", None, None),
        P("tp", None, None),
        P("tp"),
        P(REP_FS, "tp"),
        P("tp", FS),
        P(FS, "tp"),
        P("tp", FS),
    )
    return jax.shard_map(
        shards, mesh=split, in_specs=placed, out_specs=P(REP_FS, "tp"), check_vma=False
    )
```

profile of v0, /device:TPU:1, one launch (start us, length us, event | category | flops | bytes accessed | tf_op | source)
XLA Modules:
  0.0 238.8 jit_solution(2918589249318210032)
XLA Ops:
  6.5 1.6 pad_maximum_fusion.1
  8.2 19.7 %all-gather.1 = bf16[3072,128]{1,0:T(8,128)(2,1)} all-gather(bf16[768,128]{1,0:T(8,128)(2,1)} %param.25), channel_id=3, replica_groups=mesh['rep'=2,'fs_0'=4,'fs_1'=4,'tp'=8] {'fs_0'}, dimensions={0}, use_global_device_ids=true | all-gather | bytes 983040 | tf_op jit(solution)/shard_map/all_gather | solution.py:52
  27.9 0.1 copy.39
  28.1 1.6 broadcast_in_dim.20
  29.6 8.2 %all-to-all-start = ((bf16[8,512,256]{1,2,0:T(8,128)(2,1)}), bf16[8,512,256]{1,2,0:T(8,128)(2,1)S(1)}, u32[]{:S(2)}, u32[]{:S(2)}) async-start(bf16[8,512,256]{1,2,0:T(8,128)(2,1)} %broadcast_in_dim.20), calls=%async_computation | async-start | bytes 4194304 | tf_op jit(solution)/shard_map/all_to_all | solution.py:22
  37.9 22.9 %all-gather = bf16[512,768]{1,0:T(8,128)(2,1)} all-gather(bf16[128,768]{1,0:T(8,128)(2,1)S(1)} %copy-done.3), channel_id=2, replica_groups=mesh['rep'=2,'fs_0'=4,'fs_1'=4,'tp'=8] {'fs_0'}, dimensions={0}, use_global_device_ids=true | all-gather | bytes 983040 | tf_op jit(solution)/shard_map/all_gather | solution.py:52
  61.0 3.2 %all-to-all-done = bf16[8,512,256]{1,2,0:T(8,128)(2,1)S(1)} async-done(((bf16[8,512,256]{1,2,0:T(8,128)(2,1)}), bf16[8,512,256]{1,2,0:T(8,128)(2,1)S(1)}, u32[]{:S(2)}, u32[]{:S(2)}) %all-to-all-start) | async-done | bytes 2097184 | tf_op jit(solution)/shard_map/all_to_all | solution.py:22
  64.2 1.1 broadcast_in_dim.21
  65.3 6.7 %all-to-all-start.1 = ((bf16[16,256,128]{1,2,0:T(8,128)(2,1)}), bf16[16,256,128]{1,2,0:T(8,128)(2,1)S(1)}, u32[]{:S(2)}, u32[]{:S(2)}) async-start(bf16[16,256,128]{1,2,0:T(8,128)(2,1)} %broadcast_in_dim.21), calls=%async_computation.1 | async-start | bytes 2097152 | tf_op jit(solution)/shard_map/all_to_all | solution.py:22
  72.0 0.5 multiply_reduce_fusion
  72.5 1.9 fusion.4
  74.4 15.4 %all-gather.6.cloned.1.call-done = bf16[2048,512]{1,0:T(8,128)(2,1)} async-done(((bf16[128,512]{1,0:T(8,128)(2,1)}), bf16[2048,512]{1,0:T(8,128)(2,1)}) %all-gather.6.cloned.1.call-update) | async-done | bytes 2097168 | tf_op jit(solution)/shard_map/all_gather | solution.py:35
  89.8 2.6 %convolution_convert_fusion.3 = bf16[512,256]{1,0:T(8,128)(2,1)S(1)} fusion(bf16[512,2048]{0,1:T(8,128)(2,1)} %fusion.4, bf16[2048,512]{1,0:T(8,128)(2,1)} %all-gather.6.cloned.1.call-done), kind=kOutput, calls=%fused_computation.25 | convolution fusion | flops 537001984 | bytes 3407872 | tf_op jit(solution)/shard_map/dot_general | solution.py:147
  92.4 0.2 add_convert_fusion.2
  92.7 0.2 copy.40
  93.0 0.3 fusion.8
  93.4 0.2 copy.42
  93.6 0.2 copy-done.9
  93.7 0.3 fusion.10
  94.1 0.2 copy.44
  94.3 1.5 fusion.47
  95.7 0.1 slice.191
  95.9 0.1 slice.192
  96.0 0.1 slice.190
  96.2 0.8 slice.194
  97.0 1.0 fusion.57
  99.5 0.2 slice.238
  99.6 0.2 slice.189
  100.8 2.6 %convolution_convert_fusion.2 = bf16[512,256]{1,0:T(8,128)(2,1)S(1)} fusion(bf16[512,2048]{0,1:T(8,128)(2,1)} %fusion.4, bf16[2048,512]{1,0:T(8,128)(2,1)} %all-gather.6.cloned.1.call-done), kind=kOutput, calls=%fused_computation.24 | convolution fusion | flops 537001984 | bytes 3407872 | tf_op jit(solution)/shard_map/dot_general | solution.py:148
  103.5 1.2 fusion.15
  104.7 0.7 convolution_convert_fusion
  105.5 41.2 %all_to_all.25 = bf16[8,512,256]{2,1,0:T(8,128)(2,1)S(1)} all-to-all(bf16[8,512,256]{2,1,0:T(8,128)(2,1)S(1)} %bitcast.83), channel_id=1, replica_groups=mesh['rep'=2,'fs_0'=4,'fs_1'=4,'tp'=8] {'tp'}, dimensions={0} | all-to-all | bytes 4194304 | tf_op jit(solution)/shard_map/all_to_all | solution.py:45
  146.7 0.3 convert_reduce_fusion.1
  147.0 0.6 copy-done.2
  147.7 0.1 copy.47
  147.9 1.5 broadcast_in_dim.22
  149.3 4.7 %all-to-all-start.3 = ((bf16[8,512,256]{1,2,0:T(8,128)(2,1)}), bf16[8,512,256]{1,2,0:T(8,128)(2,1)S(1)}, u32[]{:S(2)}, u32[]{:S(2)}) async-start(bf16[8,512,256]{1,2,0:T(8,128)(2,1)} %broadcast_in_dim.22), calls=%async_computation.3 | async-start | bytes 4194304 | tf_op jit(solution)/shard_map/all_to_all | solution.py:22
  154.1 4.0 %copy.49 = bf16[4,4,768,128]{3,2,1,0:T(8,128)(2,1)} copy(bf16[4,4,768,128]{3,2,0,1:T(8,128)(2,1)} %bitcast.93) | data formatting | bytes 6291456 | tf_op jit(solution)/shard_map/transpose | solution.py:56
  158.1 4.7 %copy.50 = bf16[768,16,128]{0,2,1:T(8,128)(2,1)} copy(bf16[768,16,128]{2,0,1:T(8,128)(2,1)} %bitcast.81) | data formatting | bytes 6291456 | tf_op jit(solution)/shard_map/transpose | solution.py:17
  162.8 23.3 %all-gather.8.cloned.1.call-done = bf16[16,128,768]{2,1,0:T(8,128)(2,1)} async-done(((bf16[4,128,768]{2,1,0:T(8,128)(2,1)}), bf16[16,128,768]{2,1,0:T(8,128)(2,1)}) %all-gather.8.cloned.1.call-update) | async-done | bytes 3145744 | tf_op jit(solution)/shard_map/all_gather | solution.py:52
  186.1 3.9 %copy.48 = bf16[4,4,128,768]{3,2,1,0:T(8,128)(2,1)} copy(bf16[4,4,128,768]{3,2,0,1:T(8,128)(2,1)} %bitcast.94) | data formatting | bytes 6291456 | tf_op jit(solution)/shard_map/transpose | solution.py:56
  190.0 0.5 fusion
  190.5 1.9 fusion.2
  192.4 7.6 %convolution_convert_fusion.1 = bf16[512,2048]{1,0:T(8,128)(2,1)S(1)} fusion(bf16[768,2048]{0,1:T(8,128)(2,1)} %bitcast.95, bf16[512,2048]{0,1:T(8,128)(2,1)} %bitcast.101, bf16[2048,768]{1,0:T(8,128)(2,1)} %bitcast.96), kind=kOutput, calls=%fused_computation.12 | convolution fusion | flops 3223453696 | bytes 10485760 | tf_op jit(solution)/shard_map/dot_general | solution.py:175
  200.0 0.1 copy.58
  200.1 31.1 %all_to_all.26 = bf16[8,512,256]{2,1,0:T(8,128)(2,1)S(1)} all-to-all(bf16[8,512,256]{2,1,0:T(8,128)(2,1)S(1)} %bitcast.84), channel_id=1, replica_groups=mesh['rep'=2,'fs_0'=4,'fs_1'=4,'tp'=8] {'tp'}, dimensions={0} | all-to-all | bytes 4194304 | tf_op jit(solution)/shard_map/all_to_all | solution.py:45
  231.2 0.3 convert_reduce_fusion
  231.5 0.8 add_convert_fusion
  (107 shorter events, 2.8 us)
Async XLA Ops:
  6.5 86.5 %copy-start = (bf16[4,64,64]{2,1,0:T(8,128)(2,1)S(1)}, bf16[4,64,64]{2,1,0:T(8,128)(2,1)}, u32[]{:S(2)}) copy-start(bf16[4,64,64]{2,1,0:T(8,128)(2,1)} %param.19) | copy-start | bytes 98308
  6.5 21.4 %copy-start.1 = (bf16[512,256]{1,0:T(8,128)(2,1)S(1)}, bf16[512,256]{1,0:T(8,128)(2,1)}, u32[]{:S(2)}) copy-start(bf16[512,256]{1,0:T(8,128)(2,1)} %param.13) | copy-start | bytes 786436
  6.5 83.2 %all-gather.6.cloned.1.call-start = ((), (), s32[]{:S(2)}) async-start(), calls=%async_computation.5 | async-start | bytes 2228224 | tf_op jit(solution)/shard_map/all_gather | solution.py:35
  8.1 145.9 %all-gather.10.cloned.1.call-start = ((), (), s32[]{:S(2)}) async-start(), calls=%async_computation.7 | async-start | bytes 3932160 | tf_op jit(solution)/shard_map/all_gather | solution.py:52
  29.6 8.2 %copy-start.3 = (bf16[128,768]{1,0:T(8,128)(2,1)S(1)}, bf16[128,768]{1,0:T(8,128)(2,1)}, u32[]{:S(2)}) copy-start(bf16[128,768]{1,0:T(8,128)(2,1)} %param.24) | copy-start | bytes 589828
  29.6 31.2 %copy-start.4 = (bf16[256,128]{1,0:T(8,128)(2,1)S(1)}, bf16[256,128]{1,0:T(8,128)(2,1)}, u32[]{:S(2)}) copy-start(bf16[256,128]{1,0:T(8,128)(2,1)} %param.23) | copy-start | bytes 196612
  29.6 31.3 %copy-start.8 = (f32[256]{0:T(256)S(1)}, f32[256]{0:T(256)}, u32[]{:S(2)}) copy-start(f32[256]{0:T(256)} %param.21) | copy-start | bytes 3076
  29.6 31.3 %copy-start.7 = (bf16[4,256]{1,0:T(4,128)(2,1)S(1)}, bf16[4,256]{1,0:T(4,128)(2,1)}, u32[]{:S(2)}) copy-start(bf16[4,256]{1,0:T(4,128)(2,1)} %param.18) | copy-start | bytes 6148
  29.6 34.5 %all-to-all-start = ((bf16[8,512,256]{1,2,0:T(8,128)(2,1)}), bf16[8,512,256]{1,2,0:T(8,128)(2,1)S(1)}, u32[]{:S(2)}, u32[]{:S(2)}) async-start(bf16[8,512,256]{1,2,0:T(8,128)(2,1)} %broadcast_in_dim.20), calls=%async_computation | async-start | bytes 4194304 | tf_op jit(solution)/shard_map/all_to_all | solution.py:22
  37.9 148.2 %all-gather.8.cloned.1.call-start = ((), (), s32[]{:S(2)}) async-start(), calls=%async_computation.6 | async-start | bytes 3932160 | tf_op jit(solution)/shard_map/all_gather | solution.py:52
  65.2 7.2 %copy-start.5 = (f32[2048]{0:T(1024)S(1)}, f32[2048]{0:T(1024)}, u32[]{:S(2)}) copy-start(f32[2048]{0:T(1024)} %param.14) | copy-start | bytes 24580
  65.3 39.4 %all-to-all-start.1 = ((bf16[16,256,128]{1,2,0:T(8,128)(2,1)}), bf16[16,256,128]{1,2,0:T(8,128)(2,1)S(1)}, u32[]{:S(2)}, u32[]{:S(2)}) async-start(bf16[16,256,128]{1,2,0:T(8,128)(2,1)} %broadcast_in_dim.21), calls=%async_computation.1 | async-start | bytes 2097152 | tf_op jit(solution)/shard_map/all_to_all | solution.py:22
  92.9 0.8 copy-start.9
  146.7 1.0 copy-start.2
  149.3 4.7 %copy-start.6 = (f32[2048]{0:T(1024)S(1)}, f32[2048]{0:T(1024)}, u32[]{:S(2)}) copy-start(f32[2048]{0:T(1024)} %param.15) | copy-start | bytes 24580
  149.3 40.6 %all-to-all-start.3 = ((bf16[8,512,256]{1,2,0:T(8,128)(2,1)}), bf16[8,512,256]{1,2,0:T(8,128)(2,1)S(1)}, u32[]{:S(2)}, u32[]{:S(2)}) async-start(bf16[8,512,256]{1,2,0:T(8,128)(2,1)} %broadcast_in_dim.22), calls=%async_computation.3 | async-start | bytes 4194304 | tf_op jit(solution)/shard_map/all_to_all | solution.py:22
Sparse Core Ops, SparseCore 0:
  9.1 80.6 all-gather.5
  91.6 50.3 all-gather.9
  143.8 42.2 all-gather.7
where the time goes:
time: 240 us; the launch traced here: 239 us
  blocking collectives  115 us (48%)
  waiting for transfers between devices  41.9 us (17%)
  local copies, waits for them, and re-layouts  22.1 us (9%)
  starting transfers between devices  19.6 us (8%)
  matrix products  14.3 us (6%)
  between operations  13.8 us (6%)
  other arithmetic  12.3 us (5%)
    all_to_all x2, blocking collectives, sent_and_summed(): lax.all_to_all(pieces, axis, split_axis=0, concat_axis=0, tiled=True)  72.2 us
    all_gather x2, blocking collectives, gather_in_order(): pieces = lax.all_gather(pieces, axes[k], axis=0, tiled=True)  42.6 us
    all_gather x2, waiting for transfers between devices, gather_in_order(): pieces = lax.all_gather(pieces, axes[k], axis=0, tiled=True)  23.3 us
    all_to_all x3, starting transfers between devices, from_everyone(): return lax.all_to_all(copies, axis, split_axis=0, concat_axis=0, tiled=True)  19.6 us
    all_gather x1, waiting for transfers between devices, in_one_piece(): lax.all_gather(both, axis, axis=dim, tiled=True)  15.4 us
    transpose x2, local copies, waits for them, and re-layouts, gather_in_order(): pieces.transpose(*turned, *range(len(order), pieces.ndim))  7.9 us
    dot_general x1, matrix products, shards(): jnp.dot(activity, gather_axes(down_projection_weight, FS, (0, 1), 1), pre...  7.6 us
  transfers between devices with their start and end apart: 6, of which 3 were waited for; matrix products, arithmetic and copies ran while one was open for 15% of the time, Pallas kernels for 0%

commit v1 on v0

--- a/solution.py
+++ b/solution.py
@@ -49,7 +49,9 @@
 def gather_in_order(value, axes, order):
     pieces = value[None]
     for k in order:
-        pieces = lax.all_gather(pieces, axes[k], axis=0, tiled=True)
+        pieces = jnp.concatenate(
+            lax.all_to_all(jnp.stack([pieces] * lax.axis_size(axes[k])), axes[k], 0, 0), axis=0
+        )
     held = [lax.axis_size(axes[k]) for k in reversed(order)]
     pieces = pieces.reshape(*held, *value.shape)
     turned = sorted(range(len(order)), key=lambda place: order[len(order) - 1 - place])

time: 240 us -> 352 us (1.47)
  waiting for transfers between devices: 41.9 us -> 126 us
  blocking collectives: 115 us -> 80.2 us
  local copies, waits for them, and re-layouts: 22.1 us -> 56.7 us
  starting transfers between devices: 19.6 us -> 33.8 us
  other arithmetic: 12.3 us -> 23.4 us
    all_to_all x3, waiting for transfers between devices: 3.17 us -> 49.5 us  [from_everyone(): return lax.all_to_all(copies, axis, split_axis=0, concat_axis=0, tiled=True)]
    all_gather x2 -> x0, blocking collectives: 42.6 us -> none  [gather_in_order(): pieces = lax.all_gather(pieces, axes[k], axis=0, tiled=True)]
    all_to_all x0 -> x4, waiting for transfers between devices: none -> 41 us  [gather_in_order(): lax.all_to_all(jnp.stack([pieces] * lax.axis_size(axes[k])), axes[k], 0, 0)]
    all_gather x2 -> x0, waiting for transfers between devices: 23.3 us -> none  [gather_in_order(): pieces = lax.all_gather(pieces, axes[k], axis=0, tiled=True)]
    all_gather x1, waiting for transfers between devices: 15.4 us -> 35.5 us  [in_one_piece(): lax.all_gather(both, axis, axis=dim, tiled=True)]
    all_to_all x0 -> x4, starting transfers between devices: none -> 16.2 us  [gather_in_order(): lax.all_to_all(jnp.stack([pieces] * lax.axis_size(axes[k])), axes[k], 0, 0)]
    pad x12, local copies, waits for them, and re-layouts: 0.74 us -> 13.3 us  [recurrent_states(): lax.associative_scan(combine, (jnp.exp(decay_logarithm).reshape(shaped),...]
    slice x39, local copies, waits for them, and re-layouts: 2.41 us -> 14.7 us  [recurrent_states(): lax.associative_scan(combine, (jnp.exp(decay_logarithm).reshape(shaped),...]
  transfers between devices with their start and end apart: 6 -> 8, of which waited for: 3 -> 6; matrix products, arithmetic and copies ran while one was open for 15% -> 21% of each run, Pallas kernels for 0% -> 0%
where the time goes in v1:
time: 352 us; the launch traced here: 349 us
  waiting for transfers between devices  126 us (36%)
  blocking collectives  80.2 us (23%)
  local copies, waits for them, and re-layouts  56.7 us (16%)
  starting transfers between devices  33.8 us (10%)
  other arithmetic  23.4 us (7%)
  matrix products  15 us (4%)
  between operations  14 us (4%)
    all_to_all x2, blocking collectives, sent_and_summed(): lax.all_to_all(pieces, axis, split_axis=0, concat_axis=0, tiled=True)  80.2 us
    all_to_all x3, waiting for transfers between devices, from_everyone(): return lax.all_to_all(copies, axis, split_axis=0, concat_axis=0, tiled=True)  49.5 us
    all_to_all x4, waiting for transfers between devices, gather_in_order(): lax.all_to_all(jnp.stack([pieces] * lax.axis_size(axes[k])), axes[k], 0, 0)  41 us
    all_gather x1, waiting for transfers between devices, in_one_piece(): lax.all_gather(both, axis, axis=dim, tiled=True)  35.5 us
    all_to_all x3, starting transfers between devices, from_everyone(): return lax.all_to_all(copies, axis, split_axis=0, concat_axis=0, tiled=True)  17.6 us
    all_to_all x4, starting transfers between devices, gather_in_order(): lax.all_to_all(jnp.stack([pieces] * lax.axis_size(axes[k])), axes[k], 0, 0)  16.2 us
    slice x39, local copies, waits for them, and re-layouts, recurrent_states(): lax.associative_scan(combine, (jnp.exp(decay_logarithm).reshape(shaped),...  14.7 us
    pad x12, local copies, waits for them, and re-layouts, recurrent_states(): lax.associative_scan(combine, (jnp.exp(decay_logarithm).reshape(shaped),...  13.3 us
  transfers between devices with their start and end apart: 8, of which 6 were waited for; matrix products, arithmetic and copies ran while one was open for 21% of the time, Pallas kernels for 0%

profile of v1, /device:TPU:1, one launch (start us, length us, event | category | flops | bytes accessed | tf_op | source)
XLA Modules:
  0.0 349.2 jit_solution(12796438874123091280)
XLA Ops:
  6.5 1.6 pad_maximum_fusion.1
  9.2 1.5 broadcast_in_dim.6
  10.8 6.8 %all-to-all-start = ((bf16[8,512,256]{1,2,0:T(8,128)(2,1)}), bf16[8,512,256]{1,2,0:T(8,128)(2,1)S(1)}, u32[]{:S(2)}, u32[]{:S(2)}) async-start(bf16[8,512,256]{1,2,0:T(8,128)(2,1)} %broadcast_in_dim.6), calls=%async_computation | async-start | bytes 4194304 | tf_op jit(solution)/shard_map/all_to_all | solution.py:22
  17.8 26.2 %all-to-all-done = bf16[8,512,256]{1,2,0:T(8,128)(2,1)S(1)} async-done(((bf16[8,512,256]{1,2,0:T(8,128)(2,1)}), bf16[8,512,256]{1,2,0:T(8,128)(2,1)S(1)}, u32[]{:S(2)}, u32[]{:S(2)}) %all-to-all-start) | async-done | bytes 2097184 | tf_op jit(solution)/shard_map/all_to_all | solution.py:22
  44.9 4.6 %all-to-all-start.4 = ((bf16[4,1,128,768]{3,2,1,0:T(8,128)(2,1)}), bf16[4,1,128,768]{3,2,1,0:T(8,128)(2,1)S(1)}, u32[]{:S(2)}, u32[]{:S(2)}) async-start(bf16[4,1,128,768]{3,2,1,0:T(8,128)(2,1)} %stack.12), calls=%async_computation.4 | async-start | bytes 1572864 | tf_op jit(solution)/shard_map/all_to_all | solution.py:53
  50.0 1.9 fusion.4
  51.9 35.5 %all-gather.2.cloned.1.call-done = bf16[2048,512]{1,0:T(8,128)(2,1)} async-done(((bf16[128,512]{1,0:T(8,128)(2,1)}), bf16[2048,512]{1,0:T(8,128)(2,1)}) %all-gather.2.cloned.1.call-update) | async-done | bytes 2097168 | tf_op jit(solution)/shard_map/all_gather | solution.py:35
  87.4 2.6 convolution_convert_fusion.3
  90.1 1.1 stack.14
  91.2 3.5 %all-to-all-start.6 = ((bf16[4,1,768,128]{3,2,1,0:T(8,128)(2,1)}), bf16[4,1,768,128]{3,2,1,0:T(8,128)(2,1)S(1)}, u32[]{:S(2)}, u32[]{:S(2)}) async-start(bf16[4,1,768,128]{3,2,1,0:T(8,128)(2,1)} %stack.14), calls=%async_computation.6 | async-start | bytes 1572864 | tf_op jit(solution)/shard_map/all_to_all | solution.py:53
  96.5 1.5 fusion.47
  99.1 7.5 %all-to-all-done.6 = bf16[4,1,768,128]{3,2,1,0:T(8,128)(2,1)S(1)} async-done(((bf16[4,1,768,128]{3,2,1,0:T(8,128)(2,1)}), bf16[4,1,768,128]{3,2,1,0:T(8,128)(2,1)S(1)}, u32[]{:S(2)}, u32[]{:S(2)}) %all-to-all-start.6) | async-done | bytes 786464 | tf_op jit(solution)/shard_map/all_to_all | solution.py:53
  106.6 1.1 broadcast_in_dim.7
  107.7 4.9 %all-to-all-start.1 = ((bf16[16,256,128]{1,2,0:T(8,128)(2,1)}), bf16[16,256,128]{1,2,0:T(8,128)(2,1)S(1)}, u32[]{:S(2)}, u32[]{:S(2)}) async-start(bf16[16,256,128]{1,2,0:T(8,128)(2,1)} %broadcast_in_dim.7), calls=%async_computation.1 | async-start | bytes 2097152 | tf_op jit(solution)/shard_map/all_to_all | solution.py:22
  114.6 1.8 pad.51
  116.5 3.3 convolution_convert_fusion.2
  119.8 9.5 %all-to-all-done.1 = bf16[16,256,128]{1,2,0:T(8,128)(2,1)S(1)} async-done(((bf16[16,256,128]{1,2,0:T(8,128)(2,1)}), bf16[16,256,128]{1,2,0:T(8,128)(2,1)S(1)}, u32[]{:S(2)}, u32[]{:S(2)}) %all-to-all-start.1) | async-done | bytes 1048608 | tf_op jit(solution)/shard_map/all_to_all | solution.py:22
  129.3 2.2 stack.15
  131.5 3.7 %all-to-all-start.7 = ((bf16[4,4,768,128]{3,2,1,0:T(8,128)(2,1)}), bf16[4,4,768,128]{3,2,1,0:T(8,128)(2,1)S(1)}, u32[]{:S(2)}, u32[]{:S(2)}) async-start(bf16[4,4,768,128]{3,2,1,0:T(8,128)(2,1)} %stack.15), calls=%async_computation.7 | async-start | bytes 6291456 | tf_op jit(solution)/shard_map/all_to_all | solution.py:53
  135.2 1.4 fusion.51
  136.6 1.4 slice.243
  138.0 1.7 slice.189
  139.7 1.7 slice.238
  142.0 1.6 slice.195
  144.3 1.4 slice.245
  154.5 1.6 pad.58
  156.1 3.5 %pad.59 = f32[4,64,256]{2,1,0:T(8,128)} pad(f32[4,32,256]{2,1,0:T(8,128)} %add.167, f32[]{:T(128)} %constant.34.clone.1), padding=0_0_0x1_0_1x0_0_0 | pad | bytes 393220 | tf_op jit(solution)/shard_map/pad | solution.py:121
  159.6 1.7 add.169
  161.3 1.2 fusion.46
  162.5 2.2 pad.60
  164.8 3.9 %pad.61 = f32[4,128,256]{2,1,0:T(8,128)} pad(f32[4,64,256]{2,1,0:T(8,128)} %add.169, f32[]{:T(128)} %constant.34.clone.1), padding=0_0_0x1_0_1x0_0_0 | pad | bytes 786436 | tf_op jit(solution)/shard_map/pad | solution.py:121
  168.6 1.4 add.171
  170.0 1.2 fusion.15
  171.9 1.5 copy.48
  173.4 50.5 %all_to_all.45 = bf16[8,512,256]{2,1,0:T(8,128)(2,1)} all-to-all(bf16[8,512,256]{2,1,0:T(8,128)(2,1)} %bitcast.80), channel_id=1, replica_groups=mesh['rep'=2,'fs_0'=4,'fs_1'=4,'tp'=8] {'tp'}, dimensions={0} | all-to-all | bytes 4194304 | tf_op jit(solution)/shard_map/all_to_all | solution.py:45
  223.9 2.0 stack.13
  226.0 4.5 %all-to-all-start.5 = ((bf16[4,4,128,768]{3,2,1,0:T(8,128)(2,1)}), bf16[4,4,128,768]{3,2,1,0:T(8,128)(2,1)S(1)}, u32[]{:S(2)}, u32[]{:S(2)}) async-start(bf16[4,4,128,768]{3,2,1,0:T(8,128)(2,1)} %stack.13), calls=%async_computation.5 | async-start | bytes 6291456 | tf_op jit(solution)/shard_map/all_to_all | solution.py:53
  230.4 2.0 convert_reduce_fusion.1
  233.3 33.5 %all-to-all-done.5 = bf16[4,4,128,768]{3,2,1,0:T(8,128)(2,1)S(1)} async-done(((bf16[4,4,128,768]{3,2,1,0:T(8,128)(2,1)}), bf16[4,4,128,768]{3,2,1,0:T(8,128)(2,1)S(1)}, u32[]{:S(2)}, u32[]{:S(2)}) %all-to-all-start.5) | async-done | bytes 3145760 | tf_op jit(solution)/shard_map/all_to_all | solution.py:53
  266.8 2.6 broadcast_in_dim.16
  269.4 5.8 %all-to-all-start.3 = ((bf16[8,512,256]{1,2,0:T(8,128)(2,1)}), bf16[8,512,256]{1,2,0:T(8,128)(2,1)S(1)}, u32[]{:S(2)}, u32[]{:S(2)}) async-start(bf16[8,512,256]{1,2,0:T(8,128)(2,1)} %broadcast_in_dim.16), calls=%async_computation.3 | async-start | bytes 4194304 | tf_op jit(solution)/shard_map/all_to_all | solution.py:22
  275.2 3.9 %copy.38 = bf16[4,4,768,128]{3,2,0,1:T(8,128)(2,1)} copy(bf16[4,4,768,128]{3,2,1,0:T(8,128)(2,1)} %copy-done.2) | data formatting | bytes 6291456 | tf_op jit(solution)/shard_map/all_to_all | solution.py:53
  279.1 4.7 %copy.39 = bf16[768,16,128]{0,2,1:T(8,128)(2,1)} copy(bf16[768,16,128]{2,0,1:T(8,128)(2,1)} %bitcast.79) | data formatting | bytes 6291456 | tf_op jit(solution)/shard_map/transpose | solution.py:17
  283.8 3.9 %copy.37 = bf16[4,4,128,768]{3,2,0,1:T(8,128)(2,1)} copy(bf16[4,4,128,768]{3,2,1,0:T(8,128)(2,1)} %copy-done.3) | data formatting | bytes 6291456 | tf_op jit(solution)/shard_map/all_to_all | solution.py:53
  287.6 13.8 %all-to-all-done.3 = bf16[8,512,256]{1,2,0:T(8,128)(2,1)S(1)} async-done(((bf16[8,512,256]{1,2,0:T(8,128)(2,1)}), bf16[8,512,256]{1,2,0:T(8,128)(2,1)S(1)}, u32[]{:S(2)}, u32[]{:S(2)}) %all-to-all-start.3) | async-done | bytes 2097184 | tf_op jit(solution)/shard_map/all_to_all | solution.py:22
  302.0 1.9 fusion.2
  303.8 7.6 %convolution_convert_fusion.1 = bf16[512,2048]{1,0:T(8,128)(2,1)S(1)} fusion(bf16[768,2048]{0,1:T(8,128)(2,1)} %bitcast.91, bf16[512,2048]{0,1:T(8,128)(2,1)} %bitcast.97, bf16[2048,768]{1,0:T(8,128)(2,1)} %bitcast.92), kind=kOutput, calls=%fused_computation.12 | convolution fusion | flops 3223453696 | bytes 10485760 | tf_op jit(solution)/shard_map/dot_general | solution.py:177
  311.6 29.7 %all_to_all.46 = bf16[8,512,256]{2,1,0:T(8,128)(2,1)S(1)} all-to-all(bf16[8,512,256]{2,1,0:T(8,128)(2,1)S(1)} %bitcast.82), channel_id=1, replica_groups=mesh['rep'=2,'fs_0'=4,'fs_1'=4,'tp'=8] {'tp'}, dimensions={0} | all-to-all | bytes 4194304 | tf_op jit(solution)/shard_map/all_to_all | solution.py:45
  (143 shorter events, 20.9 us)
Async XLA Ops:
  6.5 88.7 %copy-start = (bf16[4,64,64]{2,1,0:T(8,128)(2,1)S(1)}, bf16[4,64,64]{2,1,0:T(8,128)(2,1)}, u32[]{:S(2)}) copy-start(bf16[4,64,64]{2,1,0:T(8,128)(2,1)} %param.20) | copy-start | bytes 98308
  6.5 80.9 %all-gather.2.cloned.1.call-start = ((), (), s32[]{:S(2)}) async-start(), calls=%async_computation.9 | async-start | bytes 2228224 | tf_op jit(solution)/shard_map/all_gather | solution.py:35
  10.7 6.9 %copy-start.18 = (bf16[256,128]{1,0:T(8,128)(2,1)S(1)}, bf16[256,128]{1,0:T(8,128)(2,1)}, u32[]{:S(2)}) copy-start(bf16[256,128]{1,0:T(8,128)(2,1)} %param.23) | copy-start | bytes 196612
  10.8 7.0 %copy-start.24 = (f32[256]{0:T(256)S(1)}, f32[256]{0:T(256)}, u32[]{:S(2)}) copy-start(f32[256]{0:T(256)} %param.21) | copy-start | bytes 3076
  10.8 7.0 %copy-start.23 = (bf16[4,256]{1,0:T(4,128)(2,1)S(1)}, bf16[4,256]{1,0:T(4,128)(2,1)}, u32[]{:S(2)}) copy-start(bf16[4,256]{1,0:T(4,128)(2,1)} %param.18) | copy-start | bytes 6148
  10.8 33.2 %copy-start.16 = (bf16[128,768]{1,0:T(8,128)(2,1)S(1)}, bf16[128,768]{1,0:T(8,128)(2,1)}, u32[]{:S(2)}) copy-start(bf16[128,768]{1,0:T(8,128)(2,1)} %param.24) | copy-start | bytes 589828
  10.8 33.2 %all-to-all-start = ((bf16[8,512,256]{1,2,0:T(8,128)(2,1)}), bf16[8,512,256]{1,2,0:T(8,128)(2,1)S(1)}, u32[]{:S(2)}, u32[]{:S(2)}) async-start(bf16[8,512,256]{1,2,0:T(8,128)(2,1)} %broadcast_in_dim.6), calls=%async_computation | async-start | bytes 4194304 | tf_op jit(solution)/shard_map/all_to_all | solution.py:22
  17.8 32.2 %copy-start.21 = (f32[2048]{0:T(1024)S(1)}, f32[2048]{0:T(1024)}, u32[]{:S(2)}) copy-start(f32[2048]{0:T(1024)} %param.14) | copy-start | bytes 24580
  44.9 45.1 %all-to-all-start.4 = ((bf16[4,1,128,768]{3,2,1,0:T(8,128)(2,1)}), bf16[4,1,128,768]{3,2,1,0:T(8,128)(2,1)S(1)}, u32[]{:S(2)}, u32[]{:S(2)}) async-start(bf16[4,1,128,768]{3,2,1,0:T(8,128)(2,1)} %stack.12), calls=%async_computation.4 | async-start | bytes 1572864 | tf_op jit(solution)/shard_map/all_to_all | solution.py:53
  51.9 38.2 %copy-start.17 = (bf16[768,128]{1,0:T(8,128)(2,1)S(1)}, bf16[768,128]{1,0:T(8,128)(2,1)}, u32[]{:S(2)}) copy-start(bf16[768,128]{1,0:T(8,128)(2,1)} %param.25) | copy-start | bytes 589828
  90.1 5.2 %copy-start.8 = (bf16[4,1,128,768]{3,2,1,0:T(8,128)(2,1)}, bf16[4,1,128,768]{3,2,1,0:T(8,128)(2,1)S(1)}, u32[]{:S(2)}) copy-start(bf16[4,1,128,768]{3,2,1,0:T(8,128)(2,1)S(1)} %all-to-all-done.4) | copy-start | bytes 2359300
  91.2 15.4 %all-to-all-start.6 = ((bf16[4,1,768,128]{3,2,1,0:T(8,128)(2,1)}), bf16[4,1,768,128]{3,2,1,0:T(8,128)(2,1)S(1)}, u32[]{:S(2)}, u32[]{:S(2)}) async-start(bf16[4,1,768,128]{3,2,1,0:T(8,128)(2,1)} %stack.14), calls=%async_computation.6 | async-start | bytes 1572864 | tf_op jit(solution)/shard_map/all_to_all | solution.py:53
  95.1 0.8 copy-start.25
  98.0 0.8 copy-start.6
  98.0 1.0 copy-start.7
  98.7 9.0 %copy-start.10 = (f32[4,64,256]{2,1,0:T(8,128)}, f32[4,64,256]{2,1,0:T(8,128)S(1)}, u32[]{:S(2)}) copy-start(f32[4,64,256]{2,1,0:T(8,128)S(1)} %get-tuple-element.7) | copy-start | bytes 786436
  107.7 21.5 %all-to-all-start.1 = ((bf16[16,256,128]{1,2,0:T(8,128)(2,1)}), bf16[16,256,128]{1,2,0:T(8,128)(2,1)S(1)}, u32[]{:S(2)}, u32[]{:S(2)}) async-start(bf16[16,256,128]{1,2,0:T(8,128)(2,1)} %broadcast_in_dim.7), calls=%async_computation.1 | async-start | bytes 2097152 | tf_op jit(solution)/shard_map/all_to_all | solution.py:22
  112.7 7.1 %copy-start.12 = (f32[4,32,256]{2,1,0:T(8,128)}, f32[4,32,256]{2,1,0:T(8,128)S(1)}, u32[]{:S(2)}) copy-start(f32[4,32,256]{2,1,0:T(8,128)S(1)} %get-tuple-element.10) | copy-start | bytes 393220
  112.7 7.0 %copy-start.13 = (f32[4,32,256]{2,1,0:T(8,128)}, f32[4,32,256]{2,1,0:T(8,128)S(1)}, u32[]{:S(2)}) copy-start(f32[4,32,256]{2,1,0:T(8,128)S(1)} %get-tuple-element.9) | copy-start | bytes 393220
  113.0 6.8 %copy-start.15 = (f32[4,8,256]{2,1,0:T(8,128)}, f32[4,8,256]{2,1,0:T(8,128)S(1)}, u32[]{:S(2)}) copy-start(f32[4,8,256]{2,1,0:T(8,128)S(1)} %get-tuple-element.14) | copy-start | bytes 98308
  129.3 2.2 copy-start.4
  131.5 41.9 %all-to-all-start.7 = ((bf16[4,4,768,128]{3,2,1,0:T(8,128)(2,1)}), bf16[4,4,768,128]{3,2,1,0:T(8,128)(2,1)S(1)}, u32[]{:S(2)}, u32[]{:S(2)}) async-start(bf16[4,4,768,128]{3,2,1,0:T(8,128)(2,1)} %stack.15), calls=%async_computation.7 | async-start | bytes 6291456 | tf_op jit(solution)/shard_map/all_to_all | solution.py:53
  149.7 4.2 %copy-start.20 = (f32[4,1,256]{2,1,0:T(1,128)S(1)}, f32[4,1,256]{2,1,0:T(1,128)}, u32[]{:S(2)}) copy-start(f32[4,1,256]{2,1,0:T(1,128)} %slice.244) | copy-start | bytes 12292
  152.1 10.4 %copy-start.19 = (f32[4,1,256]{2,1,0:T(1,128)S(1)}, f32[4,1,256]{2,1,0:T(1,128)}, u32[]{:S(2)}) copy-start(f32[4,1,256]{2,1,0:T(1,128)} %slice.243) | copy-start | bytes 12292
  164.8 5.2 %copy-start.14 = (bf16[512,256]{1,0:T(8,128)(2,1)S(1)}, bf16[512,256]{1,0:T(8,128)(2,1)}, u32[]{:S(2)}) copy-start(bf16[512,256]{1,0:T(8,128)(2,1)} %convolution_convert_fusion.2) | copy-start | bytes 786436
  168.6 2.5 copy-start.5
  173.4 50.5 %copy-start.2 = (bf16[4,4,768,128]{3,2,1,0:T(8,128)(2,1)}, bf16[4,4,768,128]{3,2,1,0:T(8,128)(2,1)S(1)}, u32[]{:S(2)}) copy-start(bf16[4,4,768,128]{3,2,1,0:T(8,128)(2,1)S(1)} %all-to-all-done.7) | copy-start | bytes 9437188
  173.4 50.5 %copy-start.9 = (bf16[4,1,128,768]{3,2,1,0:T(8,128)(2,1)S(1)}, bf16[4,1,128,768]{3,2,1,0:T(8,128)(2,1)}, u32[]{:S(2)}) copy-start(bf16[4,1,128,768]{3,2,1,0:T(8,128)(2,1)} %copy-done.8) | copy-start | bytes 2359300
  226.0 40.8 %all-to-all-start.5 = ((bf16[4,4,128,768]{3,2,1,0:T(8,128)(2,1)}), bf16[4,4,128,768]{3,2,1,0:T(8,128)(2,1)S(1)}, u32[]{:S(2)}, u32[]{:S(2)}) async-start(bf16[4,4,128,768]{3,2,1,0:T(8,128)(2,1)} %stack.13), calls=%async_computation.5 | async-start | bytes 6291456 | tf_op jit(solution)/shard_map/all_to_all | solution.py:53
  230.4 2.0 copy-start.11
  266.8 2.6 copy-start.3
  269.4 5.8 %copy-start.22 = (f32[2048]{0:T(1024)S(1)}, f32[2048]{0:T(1024)}, u32[]{:S(2)}) copy-start(f32[2048]{0:T(1024)} %param.15) | copy-start | bytes 24580
  269.4 32.0 %all-to-all-start.3 = ((bf16[8,512,256]{1,2,0:T(8,128)(2,1)}), bf16[8,512,256]{1,2,0:T(8,128)(2,1)S(1)}, u32[]{:S(2)}, u32[]{:S(2)}) async-start(bf16[8,512,256]{1,2,0:T(8,128)(2,1)} %broadcast_in_dim.16), calls=%async_computation.3 | async-start | bytes 4194304 | tf_op jit(solution)/shard_map/all_to_all | solution.py:22
  311.6 30.8 %copy-start.1 = (bf16[4,64,64]{2,1,0:T(8,128)(2,1)S(1)}, bf16[4,64,64]{2,1,0:T(8,128)(2,1)}, u32[]{:S(2)}) copy-start(bf16[4,64,64]{2,1,0:T(8,128)(2,1)} %param.20) | copy-start | bytes 98308
Sparse Core Ops, SparseCore 0:
  9.1 78.2 all-gather.1
